TPU v7x, 32 devices: a whole 2x2x4 slice. The times are simulated.
32 devices in a mesh: fs: 8 (over z, x), tp: 4 (over y, core).
Axes of the slice: x: 2, y: 2, z: 4, core: 2. Of those that a mesh axis runs over, the one named last changes fastest.
Arguments:
- prompt_tokens: bfloat16 [6144, 2048], P('fs', 'tp'), may hold values from -6 to 6
- norm_gain: float32 [2048], P('fs'), may hold values from 0.1 to 1.9
- up_master: float32 [2048, 4096], P('fs', 'tp'), may hold values from -6 to 6
- down_master: float32 [2048, 4096], P('fs', 'tp'), may hold values from -6 to 6
Outputs:
- serve_up: bfloat16 [2048, 4096], P(None, 'tp')
- serve_down: bfloat16 [2048, 4096], P(None, 'tp')
- mixed: bfloat16 [6144, 2048], P('fs', 'tp')
All inputs are finite; a program needn't handle non-finite values.
Results may differ from a plain program's by a relative error of at most 0.009.
Values may be sent and summed in bfloat16 or wider, within the bound.
A program may use at most 64 MiB of HBM per device.

v0:
```python
import jax
import jax.numpy as jnp
from jax import lax
from jax.sharding import PartitionSpec as P


def shards(prompt_tokens, norm_gain, up_master, down_master):
    up_folded = (norm_gain[:, None] * up_master).astype(jnp.bfloat16)
    down_cast = down_master.astype(jnp.bfloat16)
    whole = lax.all_gather(prompt_tokens, "tp", axis=1, tiled=True)
    width = whole.shape[1]
    hidden_units = up_master.shape[1] * lax.axis_size("tp")
    wide = whole.astype(jnp.float32)
    normed = (wide * lax.rsqrt(jnp.mean(wide * wide, axis=1, keepdims=True) + 1e-05)).astype(
        jnp.bfloat16
    )
    contract = (((1,), (1,)), ((), ()))
    serve_up, serve_down = (
        lax.all_gather(up_folded, "fs", axis=0, tiled=True),
        lax.all_gather(down_cast, "fs", axis=0, tiled=True),
    )
    hidden = jnp.dot(normed, serve_up, preferred_element_type=jnp.float32)
    act = jnp.square(jax.nn.relu(hidden * width ** (-0.5))).astype(jnp.bfloat16)
    product = lax.dot_general(act, serve_down, contract, preferred_element_type=jnp.float32)
    partial_value = (product * hidden_units ** (-0.5)).astype(jnp.bfloat16).astype(jnp.float32)
    mixed = lax.psum_scatter(
        partial_value.astype(jnp.bfloat16), "tp", scatter_dimension=1, tiled=True
    )
    return (serve_up, serve_down, mixed)


def solution(mesh):
    return jax.shard_map(
        shards,
        mesh=mesh,
        in_specs=(P("fs", "tp"), P("fs"), P("fs", "tp"), P("fs", "tp")),
        out_specs=(P(None, "tp"), P(None, "tp"), P("fs", "tp")),
        check_vma=False,
    )
```

profile of v0, /device:TPU:0, one launch (start us, length us, event | category | flops | bytes accessed | tf_op | source)
XLA Modules:
  0.0 252.3 jit_solution(355867088768193261)
XLA Ops:
  7.2 0.0 all-gather.8.cloned.1.call-start
  7.2 0.7 all-gather.8.cloned.1.call-update
  7.9 0.0 all-gather.4.cloned.1.call-start
  7.9 2.1 multiply_convert_fusion.2
  10.1 0.0 all-gather.4.cloned.1.call-update
  10.1 0.0 all-gather.6.cloned.1.call-start
  10.2 2.1 convert_element_type.21
  12.3 0.0 all-gather.6.cloned.1.call-update
  12.3 0.0 reduce-scatter.2.cloned.1.call-start
  12.3 28.5 %all-gather.8.cloned.1.call-done = bf16[768,2048]{1,0:T(8,128)(2,1)} async-done(((bf16[768,512]{1,0:T(8,128)(2,1)}), bf16[768,2048]{1,0:T(8,128)(2,1)}) %all-gather.8.cloned.1.call-update) | async-done | bytes 3145744 | tf_op jit(solution)/shard_map/all_gather | solution.py:10
  40.8 2.6 %fusion = f32[768]{0:T(1024)S(1)} fusion(bf16[768,2048]{1,0:T(8,128)(2,1)} %all-gather.8.cloned.1.call-done), kind=kLoop, calls=%fused_computation.2 | loop fusion | flops 4717824 | bytes 3148800 | tf_op jit(solution)/shard_map/reduce_sum | solution.py:14
  43.4 72.9 %all-gather.4.cloned.1.call-done = bf16[2048,1024]{1,0:T(8,128)(2,1)} async-done(((bf16[256,1024]{1,0:T(8,128)(2,1)}), bf16[2048,1024]{1,0:T(8,128)(2,1)}) %all-gather.4.cloned.1.call-update) | async-done | bytes 4194320 | tf_op jit(solution)/shard_map/all_gather | solution.py:19
  116.3 74.1 %all-gather.6.cloned.1.call-done = bf16[2048,1024]{1,0:T(8,128)(2,1)} async-done(((bf16[256,1024]{1,0:T(8,128)(2,1)}), bf16[2048,1024]{1,0:T(8,128)(2,1)}) %all-gather.6.cloned.1.call-update) | async-done | bytes 4194320 | tf_op jit(solution)/shard_map/all_gather | solution.py:20
  190.4 12.1 %multiply_convert_fusion = bf16[768,2048]{1,0:T(8,128)(2,1)} fusion(bf16[2048,1024]{1,0:T(8,128)(2,1)} %all-gather.6.cloned.1.call-done, bf16[2048,1024]{1,0:T(8,128)(2,1)} %all-gather.4.cloned.1.call-done, bf16[768,2048]{1,0:T(8,128)(2,1)} %all-gather.8.cloned.1.call-done, f32[768]{0:T(1024)S(1)} %add_rsqrt_fusion), kind=kOutput, calls=%fused_computation.4 | convolution fusion | flops 6453460992 | bytes 14683136 | tf_op jit(solution)/shard_map/dot_general | solution.py:24
  202.5 0.0 reduce-scatter.2.cloned.1.call-update
  202.5 36.4 %reduce-scatter.2.cloned.1.call-done = bf16[768,512]{1,0:T(8,128)(2,1)} async-done(((bf16[768,2048]{1,0:T(8,128)(2,1)}), bf16[768,512]{1,0:T(8,128)(2,1)}) %reduce-scatter.2.cloned.1.call-update) | async-done | bytes 786448 | tf_op jit(solution)/shard_map/reduce_scatter | solution.py:26
  238.9 0.0 copy-start
  238.9 4.8 %copy.9 = bf16[2048,1024]{1,0:T(8,128)(2,1)} copy(bf16[2048,1024]{1,0:T(8,128)(2,1)} %all-gather.4.cloned.1.call-done) | data formatting | bytes 8388608
  243.8 0.0 copy-done
  243.8 2.0 copy.10
  (1 shorter events, 0.0 us)
Async XLA Ops:
  7.2 33.6 %all-gather.8.cloned.1.call-start = ((), (), s32[]{:S(2)}) async-start(), calls=%async_computation.3 | async-start | bytes 3932160 | tf_op jit(solution)/shard_map/all_gather | solution.py:10
  7.9 108.4 %all-gather.4.cloned.1.call-start = ((), (), s32[]{:S(2)}) async-start(), calls=%async_computation.1 | async-start | bytes 4718592 | tf_op jit(solution)/shard_map/all_gather | solution.py:19
  10.1 180.3 %all-gather.6.cloned.1.call-start = ((), (), s32[]{:S(2)}) async-start(), calls=%async_computation.2 | async-start | bytes 4718592 | tf_op jit(solution)/shard_map/all_gather | solution.py:20
  12.3 226.7 %reduce-scatter.2.cloned.1.call-start = ((), (), s32[]{:S(2)}) async-start(), calls=%async_computation.4 | async-start | bytes 3932160 | tf_op jit(solution)/shard_map/reduce_scatter | solution.py:26
  238.9 4.8 %copy-start = (bf16[2048,1024]{1,0:T(8,128)(2,1)S(1)}, bf16[2048,1024]{1,0:T(8,128)(2,1)}, u32[]{:S(2)}) copy-start(bf16[2048,1024]{1,0:T(8,128)(2,1)} %all-gather.6.cloned.1.call-done) | copy-start | bytes 12582916
Sparse Core Ops, SparseCore 0:
  9.5 31.2 all-gather.7
  43.5 72.7 all-gather.3
  119.0 71.3 all-gather.5
  202.6 36.2 reduce-scatter.1
where the time goes:
time: 253 us; the launch traced here: 252 us
  waiting for transfers between devices  213 us (84%)
  between operations  13.8 us (5%)
  matrix products  12.1 us (5%)
  local copies, waits for them, and re-layouts  6.83 us (3%)
  other arithmetic  6.82 us (3%)
    all_gather x1, waiting for transfers between devices, shards(): lax.all_gather(down_cast, 'fs', axis=0, tiled=True)  74.1 us
    all_gather x1, waiting for transfers between devices, shards(): lax.all_gather(up_folded, 'fs', axis=0, tiled=True)  72.9 us
    reduce_scatter x1, waiting for transfers between devices, shards(): lax.psum_scatter(partial_value.astype(jnp.bfloat16), 'tp', scatter_dimens...  36.4 us
    all_gather x1, waiting for transfers between devices, shards(): whole = lax.all_gather(prompt_tokens, 'tp', axis=1, tiled=True)  28.5 us
    dot_general x1, matrix products, shards(): lax.dot_general(act, serve_down, contract, preferred_element_type=jnp.flo...  12.1 us
    unnamed x4, local copies, waits for them, and re-layouts  6.83 us
  transfers between devices with their start and end apart: 4, of which 4 were waited for; matrix products, arithmetic and copies ran while one was open for 3% of the time, Pallas kernels for 0%

commit v1 on v0

--- a/solution.py
+++ b/solution.py
@@ -7,7 +7,12 @@
 def shards(prompt_tokens, norm_gain, up_master, down_master):
     up_folded = (norm_gain[:, None] * up_master).astype(jnp.bfloat16)
     down_cast = down_master.astype(jnp.bfloat16)
-    whole = lax.all_gather(prompt_tokens, "tp", axis=1, tiled=True)
+    ring = [prompt_tokens]
+    for hop in range(3):
+        ring.append(lax.ppermute(ring[-1], "tp", [(dev, (dev + 1) % 4) for dev in range(4)]))
+    whole = jnp.roll(
+        jnp.concatenate(ring[::-1], axis=1), (lax.axis_index("tp") + 1) * ring[0].shape[1], axis=1
+    )
     width = whole.shape[1]
     hidden_units = up_master.shape[1] * lax.axis_size("tp")
     wide = whole.astype(jnp.float32)

time: 253 us -> 222 us (0.88)
  waiting for transfers between devices: 213 us -> 180 us
  local copies, waits for them, and re-layouts: 6.83 us -> 10.2 us
    all_gather x1, waiting for transfers between devices: 72.9 us -> 35.2 us  [shards(): lax.all_gather(up_folded, 'fs', axis=0, tiled=True)]
    ppermute x0 -> x3, waiting for transfers between devices: none -> 34.6 us  [shards(): lax.ppermute(ring[-1], 'tp', [(dev, (dev + 1) % 4) for dev in range(4)])]
    all_gather x1 -> x0, waiting for transfers between devices: 28.5 us -> none  [shards(): whole = lax.all_gather(prompt_tokens, 'tp', axis=1, tiled=True)]
    unnamed x4 -> x15, local copies, waits for them, and re-layouts: 6.83 us -> 10.1 us
  transfers between devices with their start and end apart: 4 -> 6, of which waited for: 4 -> 6; matrix products, arithmetic and copies ran while one was open for 3% -> 2% of each run, Pallas kernels for 0% -> 0%
where the time goes in v1:
time: 222 us
  waiting for transfers between devices  180 us (81%)
  between operations  13.8 us (6%)
  matrix products  12.1 us (5%)
  local copies, waits for them, and re-layouts  10.2 us (5%)
  other arithmetic  4.99 us (2%)
    all_gather x1, waiting for transfers between devices, shards(): lax.all_gather(down_cast, 'fs', axis=0, tiled=True)  74.1 us
    reduce_scatter x1, waiting for transfers between devices, shards(): lax.psum_scatter(partial_value.astype(jnp.bfloat16), 'tp', scatter_dimens...  36.4 us
    all_gather x1, waiting for transfers between devices, shards(): lax.all_gather(up_folded, 'fs', axis=0, tiled=True)  35.2 us
    ppermute x3, waiting for transfers between devices, shards(): lax.ppermute(ring[-1], 'tp', [(dev, (dev + 1) % 4) for dev in range(4)])  34.6 us
    dot_general x1, matrix products, shards(): lax.dot_general(act, serve_down, contract, preferred_element_type=jnp.flo...  12.1 us
    unnamed x15, local copies, waits for them, and re-layouts  10.1 us
  transfers between devices with their start and end apart: 6, of which 6 were waited for; matrix products, arithmetic and copies ran while one was open for 2% of the time, Pallas kernels for 0%

profile of v1, /device:TPU:0, one launch (start us, length us, event | category | flops | bytes accessed | tf_op | source)
XLA Modules:
  0.0 222.2 jit_solution(1504854416839898904)
XLA Ops:
  7.2 0.0 copy-start.1
  7.2 0.0 all-gather.3.cloned.1.call-start
  7.2 2.2 multiply_convert_fusion.2
  9.4 0.0 all-gather.3.cloned.1.call-update
  9.5 0.0 all-gather.5.cloned.1.call-start
  9.5 2.1 convert_element_type.21
  11.6 0.0 all-gather.5.cloned.1.call-update
  11.6 0.0 reduce-scatter.2.cloned.1.call-start
  11.7 0.5 collective-permute-start
  12.2 11.8 %collective-permute-done = bf16[768,512]{1,0:T(8,128)(2,1)S(1)} collective-permute-done((bf16[768,512]{1,0:T(8,128)(2,1)}, bf16[768,512]{1,0:T(8,128)(2,1)S(1)}, u32[]{:S(2)}, u32[]{:S(2)}) %collective-permute-start) | collective-permute-done | bytes 786464 | tf_op jit(solution)/shard_map/ppermute | solution.py:12
  24.0 0.0 collective-permute-start.1
  24.1 11.4 %collective-permute-done.1 = bf16[768,512]{1,0:T(8,128)(2,1)S(1)} collective-permute-done((bf16[768,512]{1,0:T(8,128)(2,1)S(1)}, bf16[768,512]{1,0:T(8,128)(2,1)S(1)}, u32[]{:S(2)}, u32[]{:S(2)}) %collective-permute-start.1) | collective-permute-done | bytes 786464 | tf_op jit(solution)/shard_map/ppermute | solution.py:12
  35.5 0.0 collective-permute-start.2
  35.5 11.4 %collective-permute-done.2 = bf16[768,512]{1,0:T(8,128)(2,1)S(1)} collective-permute-done((bf16[768,512]{1,0:T(8,128)(2,1)S(1)}, bf16[768,512]{1,0:T(8,128)(2,1)S(1)}, u32[]{:S(2)}, u32[]{:S(2)}) %collective-permute-start.2) | collective-permute-done | bytes 786464 | tf_op jit(solution)/shard_map/ppermute | solution.py:12
  46.9 0.1 constant_dynamic-update-slice_fusion.7
  47.0 0.1 constant_dynamic-update-slice_fusion.6
  47.1 0.1 constant_dynamic-update-slice_fusion.5
  47.2 0.0 copy-done.1
  47.2 0.1 constant_dynamic-update-slice_fusion.4
  47.3 0.1 constant_dynamic-update-slice_fusion.3
  47.4 0.1 constant_dynamic-update-slice_fusion.2
  47.5 0.1 constant_dynamic-update-slice_fusion.1
  47.6 0.1 constant_dynamic-update-slice_fusion
  47.7 0.0 copy-start.2
  47.7 2.7 %copy-done.2 = bf16[768,4096]{1,0:T(8,128)(2,1)} copy-done((bf16[768,4096]{1,0:T(8,128)(2,1)}, bf16[768,4096]{1,0:T(8,128)(2,1)S(1)}, u32[]{:S(2)}) %copy-start.2) | copy-done | bytes 6291480
  50.4 0.7 fusion
  51.0 35.2 %all-gather.3.cloned.1.call-done = bf16[2048,1024]{1,0:T(8,128)(2,1)} async-done(((bf16[256,1024]{1,0:T(8,128)(2,1)}), bf16[2048,1024]{1,0:T(8,128)(2,1)}) %all-gather.3.cloned.1.call-update) | async-done | bytes 4194320 | tf_op jit(solution)/shard_map/all_gather | solution.py:24
  86.2 74.1 %all-gather.5.cloned.1.call-done = bf16[2048,1024]{1,0:T(8,128)(2,1)} async-done(((bf16[256,1024]{1,0:T(8,128)(2,1)}), bf16[2048,1024]{1,0:T(8,128)(2,1)}) %all-gather.5.cloned.1.call-update) | async-done | bytes 4194320 | tf_op jit(solution)/shard_map/all_gather | solution.py:25
  160.3 12.1 %multiply_convert_fusion = bf16[768,2048]{1,0:T(8,128)(2,1)} fusion(bf16[2048,1024]{1,0:T(8,128)(2,1)} %all-gather.5.cloned.1.call-done, bf16[2048,1024]{1,0:T(8,128)(2,1)} %all-gather.3.cloned.1.call-done, f32[768]{0:T(1024)S(1)} %add_rsqrt_fusion, bf16[768,4096]{1,0:T(8,128)(2,1)} %copy-done.2, s32[]{:T(128)S(6)} %select_n.14), kind=kOutput, calls=%fused_computation.4 | convolution fusion | flops 6453460992 | bytes 14683140 | tf_op jit(solution)/shard_map/dot_general | solution.py:29
  172.4 0.0 reduce-scatter.2.cloned.1.call-update
  172.4 36.4 %reduce-scatter.2.cloned.1.call-done = bf16[768,512]{1,0:T(8,128)(2,1)} async-done(((bf16[768,2048]{1,0:T(8,128)(2,1)}), bf16[768,512]{1,0:T(8,128)(2,1)}) %reduce-scatter.2.cloned.1.call-update) | async-done | bytes 786448 | tf_op jit(solution)/shard_map/reduce_scatter | solution.py:31
  208.8 0.0 copy-start
  208.8 4.8 %copy.16 = bf16[2048,1024]{1,0:T(8,128)(2,1)} copy(bf16[2048,1024]{1,0:T(8,128)(2,1)} %all-gather.3.cloned.1.call-done) | data formatting | bytes 8388608
  213.6 0.0 copy-done
  213.6 2.0 copy.17
  (1 shorter events, 0.0 us)
Async XLA Ops:
  7.2 40.0 %copy-start.1 = (bf16[768,512]{1,0:T(8,128)(2,1)S(1)}, bf16[768,512]{1,0:T(8,128)(2,1)}, u32[]{:S(2)}) copy-start(bf16[768,512]{1,0:T(8,128)(2,1)} %param.4) | copy-start | bytes 2359300
  7.2 79.0 %all-gather.3.cloned.1.call-start = ((), (), s32[]{:S(2)}) async-start(), calls=%async_computation.1 | async-start | bytes 4718592 | tf_op jit(solution)/shard_map/all_gather | solution.py:24
  9.5 150.8 %all-gather.5.cloned.1.call-start = ((), (), s32[]{:S(2)}) async-start(), calls=%async_computation.2 | async-start | bytes 4718592 | tf_op jit(solution)/shard_map/all_gather | solution.py:25
  11.6 197.2 %reduce-scatter.2.cloned.1.call-start = ((), (), s32[]{:S(2)}) async-start(), calls=%async_computation.3 | async-start | bytes 3932160 | tf_op jit(solution)/shard_map/reduce_scatter | solution.py:31
  11.7 12.4 %collective-permute-start = (bf16[768,512]{1,0:T(8,128)(2,1)}, bf16[768,512]{1,0:T(8,128)(2,1)S(1)}, u32[]{:S(2)}, u32[]{:S(2)}) collective-permute-start(bf16[768,512]{1,0:T(8,128)(2,1)} %param.4), channel_id=1, source_target_pairs={{0,1},{1,2},{2,3},{3,0},{4,5},{5,6},{6,7},{7,4},{8,9},{9,10},{10,1... | collective-permute-start | bytes 2359304 | tf_op jit(solution)/shard_map/ppermute | solution.py:12
  24.0 11.4 %collective-permute-start.1 = (bf16[768,512]{1,0:T(8,128)(2,1)S(1)}, bf16[768,512]{1,0:T(8,128)(2,1)S(1)}, u32[]{:S(2)}, u32[]{:S(2)}) collective-permute-start(bf16[768,512]{1,0:T(8,128)(2,1)S(1)} %collective-permute-done), channel_id=1, source_target_pairs={{0,1},{1,2},{2,3},{3,0},{4,5},{5,6},{6,7},{7,4},{8,9},{9,10},{10,1... | collective-permute-start | bytes 2359304 | tf_op jit(solution)/shard_map/ppermute | solution.py:12
  35.5 11.4 %collective-permute-start.2 = (bf16[768,512]{1,0:T(8,128)(2,1)S(1)}, bf16[768,512]{1,0:T(8,128)(2,1)S(1)}, u32[]{:S(2)}, u32[]{:S(2)}) collective-permute-start(bf16[768,512]{1,0:T(8,128)(2,1)S(1)} %collective-permute-done.1), channel_id=1, source_target_pairs={{0,1},{1,2},{2,3},{3,0},{4,5},{5,6},{6,7},{7,4},{8,9},{9,10},{10,1... | collective-permute-start | bytes 2359304 | tf_op jit(solution)/shard_map/ppermute | solution.py:12
  47.7 2.7 %copy-start.2 = (bf16[768,4096]{1,0:T(8,128)(2,1)}, bf16[768,4096]{1,0:T(8,128)(2,1)S(1)}, u32[]{:S(2)}) copy-start(bf16[768,4096]{1,0:T(8,128)(2,1)S(1)} %constant_dynamic-update-slice_fusion) | copy-start | bytes 18874372
  208.8 4.8 %copy-start = (bf16[2048,1024]{1,0:T(8,128)(2,1)S(1)}, bf16[2048,1024]{1,0:T(8,128)(2,1)}, u32[]{:S(2)}) copy-start(bf16[2048,1024]{1,0:T(8,128)(2,1)} %all-gather.5.cloned.1.call-done) | copy-start | bytes 12582916
Sparse Core Ops, SparseCore 0:
  10.7 75.4 all-gather.2
  88.9 71.3 all-gather.4
  172.5 36.2 reduce-scatter.1
